TPU v7x, 32 devices: a whole 2x2x4 slice. The times are simulated.
32 devices in a mesh: sp: 16 (over z, y, x), tp: 2 (over core).
Axes of the slice: x: 2, y: 2, z: 4, core: 2. Of those that a mesh axis runs over, the one named last changes fastest.
Arguments:
- residual: bfloat16 [4096, 2048], P(('sp', 'tp')), may hold values from -6 to 6
- queries: bfloat16 [4096, 1024], P('sp', 'tp'), may hold values from -6 to 6
- keys: bfloat16 [4096, 1024], P('sp', 'tp'), may hold values from -6 to 6
- values: bfloat16 [4096, 2048], P('sp', 'tp'), may hold values from -6 to 6
- out_gate: bfloat16 [4096, 2048], P('sp', 'tp'), may hold values from -6 to 6
- in_gate: float32 [2, 4096, 8], P(None, 'sp', 'tp'), may hold values from -6 to 140, as said below
- forget_gate: float32 [2, 4096, 8], P(None, 'sp', 'tp'), may hold values from 0 to 20
- head_gain: float32 [2048], P('tp'), may hold values from 0.1 to 1.9
- w_out: bfloat16 [2048, 2048], P('tp'), may hold values from -0.125 to 0.125
- norm_gain: float32 [2048], replicated, may hold values from 0.1 to 1.9
- shared_gate: bfloat16 [2048, 512], replicated, may hold values from -0.125 to 0.125
- shared_up: bfloat16 [2048, 512], replicated, may hold values from -0.125 to 0.125
- shared_down: bfloat16 [512, 2048], replicated, may hold values from -0.25 to 0.25
- w_gate: bfloat16 [32, 2048, 512], P(('sp', 'tp')), may hold values from -0.125 to 0.125
- w_up: bfloat16 [32, 2048, 512], P(('sp', 'tp')), may hold values from -0.125 to 0.125
- w_down: bfloat16 [32, 512, 2048], P(('sp', 'tp')), may hold values from -0.25 to 0.25
- routes: int32 [4096, 4], P(('sp', 'tp')), may hold values from 0 to 31, all different within a row; in each aligned block of 128 rows (0 to 127, 128 to 255, ...) at most 32 rows name the same one
- route_weight: float32 [4096, 4], P(('sp', 'tp')), may hold values from 0.3 to 1.5
Outputs:
- layer_out: bfloat16 [4096, 2048], P(('sp', 'tp'))
Inputs may be any that keep to these rules, and one draw needn't show every extreme that they name: `in_gate`: log input gates mostly of order one. `routes`: each row names 4 different experts. Among the rows of one device (aligned blocks of 128 rows) no expert is named more than 32 times, a bound that some block reaches.
All inputs are finite; a program needn't handle non-finite values.
Results may differ from a plain program's by a relative error of at most 0.017.
Values may be sent and summed in bfloat16 or wider, within the bound.
No kernel may reach another device: no remote copies, remote signals or barrier semaphores. Data moves between devices by JAX's collectives and lax.ppermute only.
A program may use at most 128 MiB of HBM per device.

v0:
```python
import math

import jax
import jax.numpy as jnp
from jax import lax
from jax.sharding import PartitionSpec as P

epsilon = 1e-06
max_floor = -1e30


def prefix(value, axis, combine, identity, reverse):
    count, here = (lax.axis_size(axis), lax.axis_index(axis))
    everything = jax.tree.map(lambda part: lax.all_gather(part, axis), value)
    start = jax.tree.map(
        lambda part, zero: jnp.broadcast_to(jnp.asarray(zero, part.dtype), part.shape),
        value,
        identity,
    )

    def turn(k, before):
        at = count - 1 - k if reverse else k
        reached = at > here if reverse else at < here
        new = combine(before, jax.tree.map(lambda part: part[at], everything))
        return jax.tree.map(lambda a, b: jnp.where(reached, a, b), new, before)

    return lax.fori_loop(0, count, turn, start)


def combine_states(earlier, later):
    early_matrix, early_norm, early_max, early_decay = earlier
    late_matrix, late_norm, late_max, late_decay = later
    joined_max = jnp.maximum(late_decay + early_max, late_max)
    early_scale = jnp.exp(late_decay + early_max - joined_max)
    late_scale = jnp.exp(late_max - joined_max)
    joined_matrix = (
        early_scale[:, None, None] * early_matrix + late_scale[:, None, None] * late_matrix
    )
    joined_norm = early_scale[:, None] * early_norm + late_scale[:, None] * late_norm
    return (joined_matrix, joined_norm, joined_max, early_decay + late_decay)


def cell_direction(query_heads, key_heads, value_heads, gate_input, log_forget, backward):
    if backward:
        query_heads = query_heads[::-1]
        key_heads = key_heads[::-1]
        value_heads = value_heads[::-1]
        gate_input = gate_input[::-1]
        log_forget = log_forget[::-1]
    row_count, head_count, key_dim = key_heads.shape
    key_scale = 1.0 / math.sqrt(key_dim)
    running = jnp.cumsum(log_forget, axis=0)
    block_decay = running[-1]
    log_weight = block_decay[None, :] - running + gate_input
    block_max = jnp.max(log_weight, axis=0)
    scaled = jnp.exp(log_weight - block_max[None, :]) * key_scale
    weighted_keys = lax.optimization_barrier((key_heads * scaled[:, :, None]).astype(jnp.bfloat16))
    block_matrix = jnp.einsum(
        "thd,the->hde", weighted_keys, value_heads, preferred_element_type=jnp.float32
    )
    block_norm = jnp.sum(weighted_keys.astype(jnp.float32), axis=0)
    summary = (block_matrix, block_norm, block_max, block_decay)
    identity = (
        jnp.zeros_like(block_matrix),
        jnp.zeros_like(block_norm),
        jnp.full_like(block_max, max_floor),
        jnp.zeros_like(block_decay),
    )
    if backward:
        carried = prefix(summary, "sp", combine_states, identity, True)
    else:
        carried = prefix(summary, "sp", combine_states, identity, False)
    state_matrix, state_norm, state_max, unused_decay = carried
    lower = jnp.tril(jnp.ones((row_count, row_count), dtype=bool))
    running_heads = running.T
    pair_log = running_heads[:, :, None] - running_heads[:, None, :] + gate_input.T[:, None, :]
    pair_log = jnp.where(lower[None], pair_log, -jnp.inf)
    crossing_peak = running_heads + state_max[:, None]
    row_max = jnp.maximum(crossing_peak, jnp.max(pair_log, axis=2))
    scores = (
        jnp.einsum("thd,shd->hts", query_heads, key_heads, preferred_element_type=jnp.float32)
        * key_scale
    )
    cell_weight = jnp.exp(pair_log - row_max[:, :, None]) * scores
    weight_low = cell_weight.astype(jnp.bfloat16)
    inter_scale = jnp.exp(crossing_peak - row_max)
    query_wide = query_heads.astype(jnp.float32)
    read_state = jnp.einsum(
        "thd,hde->hte", query_wide, state_matrix, precision=lax.Precision.HIGHEST
    )
    read_norm = jnp.einsum("thd,hd->ht", query_wide, state_norm, precision=lax.Precision.HIGHEST)
    local_part = jnp.einsum(
        "hts,she->hte", weight_low, value_heads, preferred_element_type=jnp.float32
    )
    numerator = inter_scale[:, :, None] * read_state + local_part
    denominator = inter_scale * read_norm + jnp.sum(cell_weight, axis=2)
    result = numerator / jnp.maximum(jnp.abs(denominator), jnp.exp(-row_max))[:, :, None]
    result = jnp.transpose(result, (1, 0, 2))
    if backward:
        result = result[::-1]
    return result


def local(
    residual,
    queries,
    keys,
    values,
    out_gate,
    in_gate,
    forget_gate,
    head_gain,
    w_out,
    norm_gain,
    shared_gate,
    shared_up,
    shared_down,
    w_gate,
    w_up,
    w_down,
    routes,
    route_weight,
):
    row_count = queries.shape[0]
    local_heads = in_gate.shape[2]
    key_dim = queries.shape[1] // local_heads
    value_dim = values.shape[1] // local_heads
    query_heads = queries.reshape(row_count, local_heads, key_dim)
    key_heads = keys.reshape(row_count, local_heads, key_dim)
    value_heads = values.reshape(row_count, local_heads, value_dim)
    log_forget = jax.nn.log_sigmoid(forget_gate)
    forward_out = cell_direction(
        query_heads, key_heads, value_heads, in_gate[0], log_forget[0], False
    )
    backward_out = cell_direction(
        query_heads, key_heads, value_heads, in_gate[1], log_forget[1], True
    )
    summed = forward_out + backward_out
    normal = summed * lax.rsqrt(jnp.mean(summed * summed, axis=-1, keepdims=True) + epsilon)
    mixed_heads = (
        normal.reshape(row_count, local_heads * value_dim)
        * head_gain
        * jax.nn.sigmoid(out_gate.astype(jnp.float32))
    ).astype(jnp.bfloat16)
    own_rows = residual.shape[0]
    model_width = residual.shape[1]
    projected = lax.psum_scatter(
        jnp.dot(mixed_heads, w_out, preferred_element_type=jnp.float32).astype(jnp.bfloat16),
        "tp",
        scatter_dimension=0,
        tiled=True,
    ).astype(jnp.float32)
    updated = (residual.astype(jnp.float32) + projected).astype(jnp.bfloat16)
    updated_wide = updated.astype(jnp.float32)
    normed = (
        updated_wide
        * lax.rsqrt(jnp.mean(updated_wide * updated_wide, axis=-1, keepdims=True) + epsilon)
        * norm_gain
    ).astype(jnp.bfloat16)
    shared_expert_hidden = (
        jax.nn.silu(jnp.dot(normed, shared_gate, preferred_element_type=jnp.float32))
        * jnp.dot(normed, shared_up, preferred_element_type=jnp.float32)
    ).astype(jnp.bfloat16)
    shared = jnp.dot(shared_expert_hidden, shared_down, preferred_element_type=jnp.float32)
    expert_count = lax.axis_size("sp") * lax.axis_size("tp")
    top_count = routes.shape[1]
    capacity = own_rows * top_count * lax.axis_size("tp") // expert_count
    flat_expert = routes.reshape(own_rows * top_count)
    onehot = (flat_expert[:, None] == jnp.arange(expert_count, dtype=jnp.int32)[None, :]).astype(
        jnp.int32
    )
    position_in = jnp.sum(jnp.cumsum(onehot, axis=0) * onehot, axis=1) - 1
    slot_index = flat_expert * capacity + position_in
    source_row = jnp.arange(own_rows * top_count, dtype=jnp.int32) // top_count
    outgoing = (
        jnp.zeros((expert_count * capacity, model_width), jnp.bfloat16)
        .at[slot_index]
        .set(normed[source_row])
    )
    gate_matrix = w_gate[0]
    raising_projector = w_up[0]
    down_matrix = w_down[0]
    arrived = lax.all_to_all(
        outgoing.reshape(expert_count, capacity, model_width),
        ("sp", "tp"),
        split_axis=0,
        concat_axis=0,
        tiled=True,
    )
    source_count, slot_count, width_now = arrived.shape
    flat_rows = arrived.reshape(source_count * slot_count, width_now)
    hidden = (
        jax.nn.silu(jnp.dot(flat_rows, gate_matrix, preferred_element_type=jnp.float32))
        * jnp.dot(flat_rows, raising_projector, preferred_element_type=jnp.float32)
    ).astype(jnp.bfloat16)
    answer = jnp.dot(hidden, down_matrix, preferred_element_type=jnp.float32).astype(jnp.bfloat16)
    returned = lax.all_to_all(
        answer.reshape(source_count, slot_count, width_now),
        ("sp", "tp"),
        split_axis=0,
        concat_axis=0,
        tiled=True,
    )
    results = returned.reshape(expert_count * capacity, model_width)[slot_index]
    results = results.reshape(own_rows, top_count, model_width)
    routed = jnp.sum(results.astype(jnp.float32) * route_weight[:, :, None], axis=1)
    return (updated_wide + shared + routed).astype(jnp.bfloat16)


def solution(mesh):
    return jax.shard_map(
        local,
        mesh=mesh,
        in_specs=(
            P(("sp", "tp"), None),
            P("sp", "tp"),
            P("sp", "tp"),
            P("sp", "tp"),
            P("sp", "tp"),
            P(None, "sp", "tp"),
            P(None, "sp", "tp"),
            P("tp"),
            P("tp", None),
            P(),
            P(),
            P(),
            P(),
            P(("sp", "tp"), None, None),
            P(("sp", "tp"), None, None),
            P(("sp", "tp"), None, None),
            P(("sp", "tp"), None),
            P(("sp", "tp"), None),
        ),
        out_specs=P(("sp", "tp"), None),
        check_vma=False,
    )
```

profile of v0, /device:TPU:0, one launch (start us, length us, event | category | flops | bytes accessed | tf_op | source)
XLA Modules:
  0.0 618.9 jit_solution(13748546827381555088)
XLA Ops:
  7.6 1.2 reduce-window.24
  13.0 6.3 %rev.21 = bf16[256,4,256]{2,0,1:T(8,128)(2,1)S(1)} reverse(bf16[256,4,256]{2,0,1:T(8,128)(2,1)} %bitcast.313), dimensions={0} | reverse | bytes 1048576 | tf_op jit(solution)/shard_map/rev | solution.py:47
  22.4 1.2 reduce-window.20
  28.1 44.8 %all-reduce.2 = (f32[64]{0:T(128)S(1)}, f32[64]{0:T(128)S(1)}) all-reduce(f32[64]{0:T(128)S(1)} %dynamic-update-slice.1, f32[64]{0:T(128)S(1)} %dynamic-update-slice), channel_id=5, replica_groups=mesh['sp'=16,'tp'=2] {'sp'}, use_global_device_ids=true, to_apply=%add.1 | all-reduce | flops 128 | bytes 1024
  74.4 4.3 rev.22
  79.4 38.6 %all-gather.8 = f32[16,1,4]{2,1,0:T(1,128)} all-gather(f32[1,1,4]{2,1,0:T(1,128)S(1)} %bitcast.336), channel_id=1, replica_groups=mesh['sp'=16,'tp'=2] {'sp'}, dimensions={0}, use_global_device_ids=true | all-gather | bytes 272 | tf_op jit(solution)/shard_map/all_gather | solution.py:14
  118.0 38.7 %all-gather.6 = f32[16,1,4]{2,1,0:T(1,128)} all-gather(f32[1,1,4]{2,1,0:T(1,128)S(1)} %bitcast.337), channel_id=1, replica_groups=mesh['sp'=16,'tp'=2] {'sp'}, dimensions={0}, use_global_device_ids=true | all-gather | bytes 272 | tf_op jit(solution)/shard_map/all_gather | solution.py:14
  157.7 39.9 %all-gather.9 = f32[16,4,128]{2,1,0:T(4,128)} all-gather(f32[1,4,128]{2,1,0:T(4,128)S(1)} %bitcast.330), channel_id=7, replica_groups=mesh['sp'=16,'tp'=2] {'sp'}, dimensions={0}, use_global_device_ids=true | all-gather | bytes 34816 | tf_op jit(solution)/shard_map/all_gather | solution.py:14
  198.7 38.4 %all-gather.7 = f32[16,4,128]{2,1,0:T(4,128)S(1)} all-gather(f32[1,4,128]{2,1,0:T(4,128)S(1)} %bitcast.331), channel_id=4, replica_groups=mesh['sp'=16,'tp'=2] {'sp'}, dimensions={0}, use_global_device_ids=true | all-gather | bytes 34816 | tf_op jit(solution)/shard_map/all_gather | solution.py:14
  237.8 53.3 %while.39 = (s32[]{:T(128)}, f32[4,128,256]{2,1,0:T(8,128)S(1)}, f32[4,128]{1,0:T(4,128)S(1)}, f32[4]{0:T(128)S(1)}, s32[]{:T(128)}, /*index=5*/f32[16,4]{1,0:T(...) while((s32[]{:T(128)}, f32[4,128,256]{2,1,0:T(8,128)S(1)}, ...), condition=%wide.region_13.14_spmd.clone, body=%wide.region_12.13_spmd.clone.sunk | while | flops 657956 | bytes 1579427 | solution.py:27
  291.2 42.6 %while.38 = (s32[]{:T(128)}, f32[4,128,256]{2,1,0:T(8,128)S(1)}, f32[4,128]{1,0:T(4,128)S(1)}, f32[4]{0:T(128)S(1)}, s32[]{:T(128)}, /*index=5*/f32[16,4]{1,0:T(...) while((s32[]{:T(128)}, f32[4,128,256]{2,1,0:T(8,128)S(1)}, ...), condition=%wide.region_5.6_spmd.clone, body=%wide.region_4.5_spmd.clone.sunk | while | flops 657952 | bytes 1579365 | solution.py:27
  333.9 2.3 fusion.79
  338.1 1.3 fusion.30
  339.5 9.4 %rev.23 = f32[256,4,256]{0,2,1:T(8,128)} reverse(f32[256,4,256]{0,2,1:T(8,128)} %fusion.30), dimensions={0} | reverse | bytes 2097152 | tf_op jit(solution)/shard_map/rev | solution.py:100
  349.5 1.8 multiply_reduce_fusion.1
  351.4 1.4 copy.96
  352.8 5.0 convolution_convert_fusion.1
  358.1 1.3 reduce-window.26
  360.1 2.9 reduce-scatter.2.cloned.1.call-done
  363.0 1.3 fusion.36
  364.3 1.3 fusion.38
  365.6 12.8 %scatter_custom_fusion = bf16[1024,2048]{1,0:T(8,128)(2,1)} fusion(s32[512]{0:T(512)S(1)} %bitcast.332, bf16[128,2048]{1,0:T(8,128)(2,1)S(1)} %fusion.38, s32[1024]{0:T(1024)S(1)} %pad_clamp_fusion.1, bf16[]{:T(256)} %constant.133.clone.1), kind=kCustom, calls=%fused_computation.44 | custom fusion | bytes 4194306 | tf_op jit(solution)/shard_map/scatter | solution.py:178
  378.4 99.5 %all_to_all.10 = bf16[32,32,2048]{2,1,0:T(8,128)(2,1)S(1)} all-to-all(bf16[32,32,2048]{2,1,0:T(8,128)(2,1)} %bitcast.305), channel_id=1, replica_groups=mesh['sp'=16,'tp'=2] {'sp','tp'}, dimensions={0} | all-to-all | bytes 8388608 | tf_op jit(solution)/shard_map/all_to_all | solution.py:183
  477.8 2.0 copy-done.5
  479.8 3.7 fusion.17
  483.5 10.1 %convolution_convert_fusion = bf16[1024,2048]{1,0:T(8,128)(2,1)} fusion(bf16[1,512,2048]{2,1,0:T(8,128)(2,1)S(1)} %copy-done, f32[1024,512]{1,0:T(8,128)} %fusion.17, bf16[1024,2048]{1,0:T(8,128)(2,1)} %bitcast.308, bf16[1,2048,512]{2,1,0:T(8,128)(2,1)} %param.35), kind=kOutput, calls=%fused_computation.34 | convolution fusion | flops 4300210176 | bytes 14680064 | tf_op jit(solution)/shard_map/dot_general | solution.py:196
  493.6 4.1 all-to-all-start.1
  498.2 93.1 %all-to-all-done.1 = bf16[32,32,2048]{2,1,0:T(8,128)(2,1)} async-done(((bf16[32,32,2048]{2,1,0:T(8,128)(2,1)}), bf16[32,32,2048]{2,1,0:T(8,128)(2,1)}, u32[]{:S(2)}, u32[]{:S(2)}) %all-to-all-start.1) | async-done | bytes 4194336 | tf_op jit(solution)/shard_map/all_to_all | solution.py:197
  591.3 7.1 %gather_fusion = bf16[512,2048]{1,0:T(8,128)(2,1)S(1)} fusion(bf16[1024,2048]{1,0:T(8,128)(2,1)} %bitcast.44, s32[1024]{0:T(1024)S(1)} %pad_clamp_fusion), kind=kCustom, calls=%fused_computation.1 | custom fusion | bytes 4196352 | tf_op jit(solution)/shard_map/gather | solution.py:204
  598.5 3.0 reshape.340
  601.5 6.5 %multiply_reduce_fusion = f32[128,2048]{1,0:T(8,128)} fusion(f32[128,4,2048]{2,1,0:T(4,128)} %reshape.340, f32[128,4]{1,0:T(8,128)S(1)} %copy.101), kind=kLoop, calls=%fused_computation.33 | loop fusion | flops 1835008 | bytes 5244928 | tf_op jit(solution)/shard_map/reduce_sum | solution.py:206
  608.0 4.4 fusion.15
  (265 shorter events, 117.0 us)
Async XLA Ops:
  6.5 477.0 %copy-start = (bf16[1,512,2048]{2,1,0:T(8,128)(2,1)S(1)}, bf16[1,512,2048]{2,1,0:T(8,128)(2,1)}, u32[]{:S(2)}) copy-start(bf16[1,512,2048]{2,1,0:T(8,128)(2,1)} %param.37) | copy-start | bytes 6291460
  6.5 5.6 copy-start.11
  6.5 231.3 %all-gather.15.cloned.1.call-start = ((), (), s32[]{:S(2)}) async-start(), calls=%async_computation.5 | async-start | bytes 8912896 | tf_op jit(solution)/shard_map/all_gather | solution.py:14
  11.9 1.1 copy-start.15
  12.1 10.3 %copy-start.8 = (bf16[256,4,128]{2,0,1:T(8,128)(2,1)}, bf16[256,4,128]{2,0,1:T(8,128)(2,1)S(1)}, u32[]{:S(2)}) copy-start(bf16[256,4,128]{2,0,1:T(8,128)(2,1)S(1)} %multiply_convert_fusion.3) | copy-start | bytes 786436
  12.1 12.1 %copy-start.17 = (f32[2,256,4]{1,2,0:T(4,128)S(1)}, f32[2,256,4]{1,2,0:T(4,128)}, u32[]{:S(2)}) copy-start(f32[2,256,4]{1,2,0:T(4,128)} %param.27) | copy-start | bytes 24580
  19.3 0.8 copy-start.13
  20.1 6.3 %copy-start.23 = (u32[32]{0:T(128)S(1)}, u32[32]{0:T(128)}, u32[]{:S(2)}) copy-start(u32[32]{0:T(128)} %constant.146) | copy-start | bytes 388
  21.2 52.5 %copy-start.6 = (bf16[256,512]{1,0:T(8,128)(2,1)S(1)}, bf16[256,512]{1,0:T(8,128)(2,1)}, u32[]{:S(2)}) copy-start(bf16[256,512]{1,0:T(8,128)(2,1)} %param.23) | copy-start | bytes 786436
  21.2 270.0 %all-gather.13.cloned.1.call-start = ((), (), s32[]{:S(2)}) async-start(), calls=%async_computation.4 | async-start | bytes 8912896 | tf_op jit(solution)/shard_map/all_gather | solution.py:14
  24.5 0.7 copy-start.9
  26.3 336.7 %reduce-scatter.2.cloned.1.call-start = ((), (), s32[]{:S(2)}) async-start(), calls=%async_computation.3 | async-start | bytes 1572864 | tf_op jit(solution)/shard_map/reduce_scatter | solution.py:147
  333.8 2.4 copy-start.7
  333.8 2.4 copy-start.16
  336.2 1.9 copy-start.14
  339.5 10.0 %copy-start.12 = (bf16[256,1024]{1,0:T(8,128)(2,1)S(1)}, bf16[256,1024]{1,0:T(8,128)(2,1)}, u32[]{:S(2)}) copy-start(bf16[256,1024]{1,0:T(8,128)(2,1)} %param.25) | copy-start | bytes 1572868
  351.3 1.5 copy-start.22
  352.8 5.0 copy-start.19
  357.7 5.2 copy-start.2
  357.7 6.6 %copy-start.18 = (f32[2048]{0:T(1024)S(1)}, f32[2048]{0:T(1024)}, u32[]{:S(2)}) copy-start(f32[2048]{0:T(1024)} %param.31) | copy-start | bytes 24580
  365.6 132.2 %copy-start.4 = (bf16[128,2048]{1,0:T(8,128)(2,1)}, bf16[128,2048]{1,0:T(8,128)(2,1)S(1)}, u32[]{:S(2)}) copy-start(bf16[128,2048]{1,0:T(8,128)(2,1)S(1)} %fusion.38) | copy-start | bytes 1572868
  378.4 101.4 %copy-start.21 = (bf16[1,2048,512]{2,1,0:T(8,128)(2,1)S(1)}, bf16[1,2048,512]{2,1,0:T(8,128)(2,1)}, u32[]{:S(2)}) copy-start(bf16[1,2048,512]{2,1,0:T(8,128)(2,1)} %param.36) | copy-start | bytes 6291460
  477.8 2.0 copy-start.5
  493.6 4.1 copy-start.20
  493.6 4.2 copy-start.10
  493.6 97.7 %all-to-all-start.1 = ((bf16[32,32,2048]{2,1,0:T(8,128)(2,1)}), bf16[32,32,2048]{2,1,0:T(8,128)(2,1)}, u32[]{:S(2)}, u32[]{:S(2)}) async-start(bf16[32,32,2048]{2,1,0:T(8,128)(2,1)} %bitcast.306), calls=%async_computation.2 | async-start | bytes 8388608 | tf_op jit(solution)/shard_map/all_to_all | solution.py:197
  601.5 6.5 %copy-start.3 = (bf16[128,2048]{1,0:T(8,128)(2,1)S(1)}, bf16[128,2048]{1,0:T(8,128)(2,1)}, u32[]{:S(2)}) copy-start(bf16[128,2048]{1,0:T(8,128)(2,1)} %reduce-scatter.2.cloned.1.call-done) | copy-start | bytes 1572868
  601.5 10.9 %copy-start.1 = (bf16[1,512,2048]{2,1,0:T(8,128)(2,1)S(1)}, bf16[1,512,2048]{2,1,0:T(8,128)(2,1)}, u32[]{:S(2)}) copy-start(bf16[1,512,2048]{2,1,0:T(8,128)(2,1)} %param.37) | copy-start | bytes 6291460
Sparse Core Ops, SparseCore 0:
  21.3 115.7 all-gather.14
  139.9 111.1 all-gather.12
  357.9 5.0 reduce-scatter.1
where the time goes:
time: 625 us; the launch traced here: 619 us
  blocking collectives  300 us (48%)
  other arithmetic  114 us (18%)
  waiting for transfers between devices  96 us (15%)
  local copies, waits for them, and re-layouts  57.3 us (9%)
  matrix products  33.5 us (5%)
  between operations  14.2 us (2%)
    all_gather x4, blocking collectives, prefix(): everything = jax.tree.map(lambda part: lax.all_gather(part, axis), value)  156 us
    all_to_all x1, blocking collectives, local(): lax.all_to_all(outgoing.reshape(expert_count, capacity, model_width), ('s...  99.5 us
    all_to_all x1, waiting for transfers between devices, local(): lax.all_to_all(answer.reshape(source_count, slot_count, width_now), ('sp'...  93.1 us
    select_n x96, other arithmetic, turn(): return jax.tree.map(lambda a, b: jnp.where(reached, a, b), new, before)  74 us
    unnamed x1, blocking collectives  44.8 us
    exp x32, other arithmetic, combine_states(): early_scale = jnp.exp(late_decay + early_max - joined_max)  21.9 us
    scatter x1, local copies, waits for them, and re-layouts, local(): outgoing = jnp.zeros((expert_count * capacity, model_width), jnp.bfloat16...  12.8 us
  transfers between devices with their start and end apart: 4, of which 2 were waited for; matrix products, arithmetic and copies ran while one was open for 11% of the time, Pallas kernels for 0%

commit v1 on v0

v1 whole, which is shorter than its diff:
```python
import functools
import math

import jax
import jax.numpy as jnp
from jax import lax
from jax.experimental import pallas as pl
from jax.experimental.pallas import tpu as pltpu
from jax.sharding import PartitionSpec as P

epsilon = 1e-06
max_floor = -1e30
stat_rows = 16
f32 = jnp.float32
bf16 = jnp.bfloat16


def three_parts(wide):
    high = wide.astype(bf16).astype(f32)
    rest = wide - high
    middle = rest.astype(bf16).astype(f32)
    return (high, middle, rest - middle)


def pack_stats(norm, first, second):
    row = lax.broadcasted_iota(jnp.int32, (stat_rows, norm.shape[1]), 0)
    left = jnp.zeros(row.shape, f32)
    right = jnp.zeros(row.shape, f32)
    for at, part in enumerate(three_parts(norm)):
        left = jnp.where(row == at, part, left)
    for at, part in enumerate(three_parts(first) + three_parts(second)):
        right = jnp.where(row == at, part, right)
    return jnp.concatenate([left, right], axis=1).astype(bf16)


def sum_parts(tile, start, low, high):
    wide = tile[start : start + 3, low:high]
    return wide[0:1] + wide[1:2] + wide[2:3]


def triangles(rows):
    row = lax.broadcasted_iota(jnp.int32, (rows, rows), 0)
    column = lax.broadcasted_iota(jnp.int32, (rows, rows), 1)
    return (column <= row, column >= row)


def exact_dot(a, b):
    return lax.dot_general(
        a, b, (((1,), (0,)), ((), ())), precision=lax.Precision.HIGHEST, preferred_element_type=f32
    )


def running_columns(forget, heads):
    lower, upper = triangles(forget.shape[0])
    column = lax.broadcasted_iota(jnp.int32, forget.shape, 1)
    return jnp.where(
        column < heads,
        exact_dot(lower.astype(f32), forget),
        exact_dot(upper.astype(f32), forget),
    )


def summary_kernel(forget, gate, keys, values, out, *, heads, key_dim, value_dim, piece):
    rows = keys.shape[0]
    running = running_columns(forget[...], heads)
    column = lax.broadcasted_iota(jnp.int32, (1, 2 * heads), 1)
    total = jnp.where(column < heads, running[rows - 1 : rows], running[0:1])
    log_weight = total - running + gate[...]
    block_max = jnp.max(log_weight, axis=0, keepdims=True)
    scaled = jnp.exp(log_weight - block_max) * (1.0 / math.sqrt(key_dim))
    for pair in range(2 * heads):
        h = pair % heads
        key = keys[:, h * key_dim : (h + 1) * key_dim].astype(f32)
        weighted = (key * scaled[:, pair : pair + 1]).astype(bf16)
        matrix = lax.dot_general(
            weighted,
            values[:, h * value_dim : (h + 1) * value_dim],
            (((0,), (0,)), ((), ())),
            preferred_element_type=f32,
        ).astype(bf16)
        norm = jnp.sum(weighted.astype(f32), axis=0, keepdims=True)
        wide = (1, key_dim)
        tile = pack_stats(
            norm,
            jnp.broadcast_to(block_max[:, pair : pair + 1], wide),
            jnp.broadcast_to(total[:, pair : pair + 1], wide),
        )
        count = key_dim // piece
        for s in range(count):
            out[pair * count + s, 0:piece, :] = matrix[s * piece : (s + 1) * piece]
            out[pair * count + s, piece : piece + stat_rows, :] = tile


def prefix_kernel(backward, blocks, out, *, piece, key_dim):
    count = blocks.shape[0]
    width = blocks.shape[2]

    def step(k, before):
        matrix, norm, peak = before
        at = jnp.where(backward[0] != 0, count - 1 - k, k)
        out[at, 0:piece, :] = matrix.astype(bf16)
        out[at, piece : piece + stat_rows, :] = pack_stats(norm, peak, peak)
        tile = blocks[at, piece : piece + stat_rows, :].astype(f32)
        block_norm = sum_parts(tile, 0, 0, key_dim)
        block_max = sum_parts(tile, 0, key_dim, width)
        total = sum_parts(tile, 3, key_dim, width)
        joined = jnp.maximum(total + peak, block_max)
        keep = jnp.exp(total + peak - joined)
        add = jnp.exp(block_max - joined)
        wide_keep = jnp.concatenate([keep] * (width // key_dim), axis=1)
        wide_add = jnp.concatenate([add] * (width // key_dim), axis=1)
        matrix = wide_keep * matrix + wide_add * blocks[at, 0:piece, :].astype(f32)
        return (matrix, keep * norm + add * block_norm, joined)

    lax.fori_loop(
        0,
        count,
        step,
        (
            jnp.zeros((piece, width), f32),
            jnp.zeros((1, key_dim), f32),
            jnp.full((1, key_dim), max_floor, f32),
        ),
    )


def cell_kernel(
    forget, gate, forget_row, gate_row, queries, keys, values, out_gate, gain, states, out,
    *, heads, key_dim, value_dim, piece,
):
    rows = keys.shape[0]
    key_scale = 1.0 / math.sqrt(key_dim)
    running = running_columns(forget[...], heads)
    lower, upper = triangles(rows)
    side = lax.broadcasted_iota(jnp.int32, (2 * heads, rows), 0)
    running_row = jnp.where(
        side < heads,
        exact_dot(forget_row[...], upper.astype(f32)),
        exact_dot(forget_row[...], lower.astype(f32)),
    )
    source = gate_row[...] - running_row
    count = key_dim // piece
    for h in range(heads):
        query = queries[:, h * key_dim : (h + 1) * key_dim]
        value = values[:, h * value_dim : (h + 1) * value_dim]
        scores = lax.dot_general(
            query,
            keys[:, h * key_dim : (h + 1) * key_dim],
            (((1,), (1,)), ((), ())),
            preferred_element_type=f32,
        ) * key_scale
        summed = None
        for direction in range(2):
            pair = direction * heads + h
            tile = states[pair * count, piece : piece + stat_rows, :].astype(f32)
            norm = sum_parts(tile, 0, 0, key_dim)
            peak = sum_parts(tile, 0, key_dim, 2 * key_dim)[:, 0:1]
            matrix = jnp.concatenate(
                [states[pair * count + s, 0:piece, :] for s in range(count)], axis=0
            )
            here = running[:, pair : pair + 1]
            pair_log = jnp.where(
                upper if direction else lower, here + source[pair : pair + 1, :], -jnp.inf
            )
            crossing = here + peak
            row_max = jnp.maximum(crossing, jnp.max(pair_log, axis=1, keepdims=True))
            weight = jnp.exp(pair_log - row_max) * scores
            carry = jnp.exp(crossing - row_max)
            read_state = jnp.dot(query, matrix, preferred_element_type=f32)
            read_norm = jnp.sum(query.astype(f32) * norm, axis=1, keepdims=True)
            local_part = jnp.dot(weight.astype(bf16), value, preferred_element_type=f32)
            divisor = carry * read_norm + jnp.sum(weight, axis=1, keepdims=True)
            divisor = jnp.maximum(jnp.abs(divisor), jnp.exp(-row_max))
            result = (carry * read_state + local_part) / divisor
            summed = result if summed is None else summed + result
        normal = summed * lax.rsqrt(jnp.mean(summed * summed, axis=1, keepdims=True) + epsilon)
        columns = slice(h * value_dim, (h + 1) * value_dim)
        out[:, columns] = (
            normal * gain[:, columns] * jax.nn.sigmoid(out_gate[:, columns].astype(f32))
        ).astype(bf16)


def mixer(queries, keys, values, out_gate, in_gate, forget_gate, head_gain):
    rows = queries.shape[0]
    heads = in_gate.shape[2]
    key_dim = queries.shape[1] // heads
    value_dim = values.shape[1] // heads
    count = lax.axis_size("sp")
    piece = 2 * heads * key_dim // count
    log_forget = jax.nn.log_sigmoid(forget_gate)
    forget = jnp.transpose(log_forget, (1, 0, 2)).reshape(rows, 2 * heads)
    gate = jnp.transpose(in_gate, (1, 0, 2)).reshape(rows, 2 * heads)
    forget_row = jnp.transpose(log_forget, (0, 2, 1)).reshape(2 * heads, rows)
    gate_row = jnp.transpose(in_gate, (0, 2, 1)).reshape(2 * heads, rows)
    sizes = dict(heads=heads, key_dim=key_dim, value_dim=value_dim, piece=piece)
    shape = jax.ShapeDtypeStruct((count, piece + stat_rows, value_dim), bf16)
    in_vmem = pl.BlockSpec(memory_space=pltpu.VMEM)
    summary = pl.pallas_call(
        functools.partial(summary_kernel, **sizes), out_shape=shape, name="summary"
    )(forget, gate, keys, values)
    blocks = lax.all_to_all(summary, "sp", split_axis=0, concat_axis=0, tiled=True)
    backward = (lax.axis_index("sp") * piece // key_dim >= heads).astype(jnp.int32).reshape(1)
    entering = pl.pallas_call(
        functools.partial(prefix_kernel, piece=piece, key_dim=key_dim),
        out_shape=shape,
        in_specs=[pl.BlockSpec(memory_space=pltpu.SMEM), in_vmem],
        name="prefix",
    )(backward, blocks)
    states = lax.all_to_all(entering, "sp", split_axis=0, concat_axis=0, tiled=True)
    return pl.pallas_call(
        functools.partial(cell_kernel, **sizes),
        out_shape=jax.ShapeDtypeStruct(values.shape, bf16),
        name="cell",
    )(
        forget, gate, forget_row, gate_row, queries, keys, values, out_gate,
        head_gain.reshape(1, -1), states,
    )


def routing(routes, route_weight, expert_count, capacity):
    rows = routes.shape[0]
    slots = expert_count * capacity
    named = routes[:, :, None] == jnp.arange(expert_count, dtype=jnp.int32)
    member = jnp.any(named, axis=1).astype(bf16)
    weight = jnp.sum(jnp.where(named, route_weight[:, :, None], 0.0), axis=1)
    row = lax.broadcasted_iota(jnp.int32, (rows, rows), 0)
    column = lax.broadcasted_iota(jnp.int32, (rows, rows), 1)
    rank = jnp.dot((column < row).astype(bf16), member, preferred_element_type=f32)
    expert = lax.broadcasted_iota(jnp.int32, (expert_count, slots), 0)
    slot = lax.broadcasted_iota(jnp.int32, (expert_count, slots), 1)
    spread = slot // capacity == expert
    wide = functools.partial(jnp.dot, preferred_element_type=f32)
    rank_key = jnp.where(member > 0, rank, float(rows)).astype(bf16)
    place = (jnp.arange(slots, dtype=jnp.int32) % capacity).astype(f32)
    hit = wide(rank_key, spread.astype(bf16)) == place
    weights = lax.dot_general(
        weight, spread.astype(f32), (((1,), (0,)), ((), ())),
        precision=lax.Precision.HIGHEST, preferred_element_type=f32,
    )
    weights = jnp.where(hit, weights, 0.0)
    return hit.astype(bf16), weights


def two_parts(weights):
    high = lax.reduce_precision(weights, 8, 7)
    return high.astype(bf16), (weights - high).astype(bf16)


def expert_layer(rows_in, gate_matrix, up_matrix, down_matrix):
    hidden = (
        jax.nn.silu(jnp.dot(rows_in, gate_matrix, preferred_element_type=f32))
        * jnp.dot(rows_in, up_matrix, preferred_element_type=f32)
    ).astype(bf16)
    return jnp.dot(hidden, down_matrix, preferred_element_type=f32)


def local(
    residual,
    queries,
    keys,
    values,
    out_gate,
    in_gate,
    forget_gate,
    head_gain,
    w_out,
    norm_gain,
    shared_gate,
    shared_up,
    shared_down,
    w_gate,
    w_up,
    w_down,
    routes,
    route_weight,
):
    own_rows, model_width = residual.shape
    mixed_heads = mixer(queries, keys, values, out_gate, in_gate, forget_gate, head_gain)
    part = jnp.dot(mixed_heads, w_out, preferred_element_type=f32).astype(bf16)
    side = lax.axis_index("tp")
    pairs = [(0, 1), (1, 0)]
    other = lax.dynamic_slice_in_dim(part, (1 - side) * own_rows, own_rows)
    kept = lax.dynamic_slice_in_dim(part, side * own_rows, own_rows)
    projected = kept.astype(f32) + lax.ppermute(other, "tp", pairs).astype(f32)
    updated = (residual.astype(f32) + projected).astype(bf16)
    updated_wide = updated.astype(f32)
    normed = (
        updated_wide
        * lax.rsqrt(jnp.mean(updated_wide * updated_wide, axis=-1, keepdims=True) + epsilon)
        * norm_gain
    ).astype(bf16)
    expert_count = lax.axis_size("sp") * lax.axis_size("tp")
    capacity = own_rows * routes.shape[1] * lax.axis_size("tp") // expert_count
    hit, weights = routing(routes, route_weight, expert_count, capacity)
    outgoing = lax.dot_general(
        hit, normed, (((0,), (0,)), ((), ())), preferred_element_type=f32
    ).astype(bf16)
    arrived = lax.all_to_all(
        outgoing.reshape(expert_count, capacity, model_width),
        ("sp", "tp"), split_axis=0, concat_axis=0, tiled=True,
    )
    shared = expert_layer(normed, shared_gate, shared_up, shared_down)
    answer = expert_layer(
        arrived.reshape(expert_count * capacity, model_width), w_gate[0], w_up[0], w_down[0]
    ).astype(bf16)
    returned = lax.all_to_all(
        answer.reshape(expert_count, capacity, model_width),
        ("sp", "tp"), split_axis=0, concat_axis=0, tiled=True,
    ).reshape(expert_count * capacity, model_width)
    high, low = two_parts(weights)
    routed = jnp.dot(high, returned, preferred_element_type=f32) + jnp.dot(
        low, returned, preferred_element_type=f32
    )
    return (updated_wide + shared + routed).astype(bf16)


def solution(mesh):
    return jax.shard_map(
        local,
        mesh=mesh,
        in_specs=(
            P(("sp", "tp"), None),
            P("sp", "tp"),
            P("sp", "tp"),
            P("sp", "tp"),
            P("sp", "tp"),
            P(None, "sp", "tp"),
            P(None, "sp", "tp"),
            P("tp"),
            P("tp", None),
            P(),
            P(),
            P(),
            P(),
            P(("sp", "tp"), None, None),
            P(("sp", "tp"), None, None),
            P(("sp", "tp"), None, None),
            P(("sp", "tp"), None),
            P(("sp", "tp"), None),
        ),
        out_specs=P(("sp", "tp"), None),
        check_vma=False,
    )
```

time: 625 us -> 291 us (0.47)
  blocking collectives: 300 us -> 96.9 us
  other arithmetic: 114 us -> 2.45 us
  local copies, waits for them, and re-layouts: 57.3 us -> 8.19 us
  waiting for transfers between devices: 96 us -> 121 us
  between operations: 14.2 us -> 0.22 us
  starting transfers between devices: 4.14 us -> 16.8 us
  Pallas kernels: 0 us -> 12.1 us
    all_gather x4 -> x0, blocking collectives: 156 us -> none  [prefix(): everything = jax.tree.map(lambda part: lax.all_gather(part, axis), value)]
    select_n x98 -> x0, other arithmetic: 74 us -> none  [the longest x96 74 us: turn(): return jax.tree.map(lambda a, b: jnp.where(reached, a, b), new, before)]
    unnamed x1 -> x0, blocking collectives: 44.8 us -> none
    all_to_all x1 -> x3, waiting for transfers between devices: 93.1 us -> 120 us  [the longest x1 86.9 us: local(): lax.all_to_all(answer.reshape(expert_count, capacity, model_width), ('sp'...]
    exp x32 -> x0, other arithmetic: 21.9 us -> none  [combine_states(): early_scale = jnp.exp(late_decay + early_max - joined_max)]
    rev x6 -> x0, local copies, waits for them, and re-layouts: 20.7 us -> none  [the longest x1 9.38 us: cell_direction(): result = result[::-1]]
    scatter x1 -> x0, local copies, waits for them, and re-layouts: 12.8 us -> none  [local(): outgoing = jnp.zeros((expert_count * capacity, model_width), jnp.bfloat16...]
    all_to_all x1 -> x3, starting transfers between devices: 4.06 us -> 16.7 us  [the longest x1 8.47 us: mixer(): lax.all_to_all(summary, 'sp', split_axis=0, concat_axis=0, tiled=True)]
  transfers between devices with their start and end apart: 4 -> 4, of which waited for: 2 -> 4; matrix products, arithmetic and copies ran while one was open for 11% -> 3% of each run, Pallas kernels for 0% -> 0%
where the time goes in v1:
time: 291 us; the launch traced here: 290 us
  waiting for transfers between devices  121 us (42%)
  blocking collectives  96.9 us (33%)
  matrix products  32.7 us (11%)
  starting transfers between devices  16.8 us (6%)
  Pallas kernels  12.1 us (4%)
  local copies, waits for them, and re-layouts  8.19 us (3%)
    all_to_all x1, blocking collectives, local(): lax.all_to_all(outgoing.reshape(expert_count, capacity, model_width), ('s...  96.9 us
    all_to_all x1, waiting for transfers between devices, local(): lax.all_to_all(answer.reshape(expert_count, capacity, model_width), ('sp'...  86.9 us
    all_to_all x1, waiting for transfers between devices, mixer(): lax.all_to_all(summary, 'sp', split_axis=0, concat_axis=0, tiled=True)  17.3 us
    all_to_all x1, waiting for transfers between devices, mixer(): lax.all_to_all(entering, 'sp', split_axis=0, concat_axis=0, tiled=True)  15.2 us
    dot_general x2, matrix products, expert_layer(): return jnp.dot(hidden, down_matrix, preferred_element_type=f32)  14.3 us
    all_to_all x1, starting transfers between devices, mixer(): lax.all_to_all(summary, 'sp', split_axis=0, concat_axis=0, tiled=True)  8.47 us
    pallas_call x1, Pallas kernels, mixer(): pl.pallas_call(functools.partial(cell_kernel, **sizes), out_shape=jax.Sha...  6.36 us
  transfers between devices with their start and end apart: 4, of which 4 were waited for; matrix products, arithmetic and copies ran while one was open for 3% of the time, Pallas kernels for 0%

profile of v1, /device:TPU:0, one launch (start us, length us, event | category | flops | bytes accessed | tf_op | source)
XLA Modules:
  0.0 290.4 jit_solution(18351926949184895620)
XLA Ops:
  0.0 0.9 fusion.62
  0.9 0.8 copy.31.forget
  1.7 0.7 reshape.54
  2.4 0.8 copy.32.gate
  3.2 3.4 %summary.1 = bf16[16,80,256]{2,1,0:T(8,128)(2,1)} custom-call(f32[256,8]{1,0:T(8,128)} %copy.31.forget, f32[256,8]{1,0:T(8,128)} %copy.32.gate, bf16[256,512]{1,0:T(8,128)(2,1)} %keys.3, bf16[256,1024]{1,0:T(8,128)(2,1)} %values.3), custom_call_target="tpu_custom_call" | custom-call | tf_op jit(solution)/shard_map/summary/pallas_call | solution.py:198
  6.5 8.5 %all-to-all-start = ((bf16[16,80,256]{2,1,0:T(8,128)(2,1)}), bf16[16,80,256]{2,1,0:T(8,128)(2,1)S(1)}, u32[]{:S(2)}, u32[]{:S(2)}) async-start(bf16[16,80,256]{2,1,0:T(8,128)(2,1)} %summary.1), calls=%async_computation | async-start | bytes 1310720 | tf_op jit(solution)/shard_map/all_to_all | solution.py:201
  15.0 17.3 %all-to-all-done.blocks = bf16[16,80,256]{2,1,0:T(8,128)(2,1)S(1)} async-done(((bf16[16,80,256]{2,1,0:T(8,128)(2,1)}), bf16[16,80,256]{2,1,0:T(8,128)(2,1)S(1)}, u32[]{:S(2)}, u32[]{:S(2)}) %all-to-all-start) | async-done | bytes 655392 | tf_op jit(solution)/shard_map/all_to_all | solution.py:201
  32.4 0.9 copy-done.3
  33.2 2.4 prefix.1
  35.6 4.5 %all-to-all-start.1 = ((bf16[16,80,256]{2,1,0:T(8,128)(2,1)}), bf16[16,80,256]{2,1,0:T(8,128)(2,1)S(1)}, u32[]{:S(2)}, u32[]{:S(2)}) async-start(bf16[16,80,256]{2,1,0:T(8,128)(2,1)} %prefix.1), calls=%async_computation.1 | async-start | bytes 1310720 | tf_op jit(solution)/shard_map/all_to_all | solution.py:209
  40.1 0.6 reshape.55.forget_row
  40.7 0.6 reshape.56.gate_row
  41.3 15.2 %all-to-all-done.1.states = bf16[16,80,256]{2,1,0:T(8,128)(2,1)S(1)} async-done(((bf16[16,80,256]{2,1,0:T(8,128)(2,1)}), bf16[16,80,256]{2,1,0:T(8,128)(2,1)S(1)}, u32[]{:S(2)}, u32[]{:S(2)}) %all-to-all-start.1) | async-done | bytes 655392 | tf_op jit(solution)/shard_map/all_to_all | solution.py:209
  56.6 0.8 copy-done.4
  57.4 6.4 %cell.1 = bf16[256,1024]{1,0:T(8,128)(2,1)} custom-call(f32[256,8]{1,0:T(8,128)} %copy.31.forget, f32[256,8]{1,0:T(8,128)} %copy.32.gate, f32[8,256]{1,0:T(8,128)} %reshape.55.forget_row, f32[8,256]{1,0:T(8,128)} %reshape.56.gate_row, bf16[256,512]{1,0:T(8,128)(2,1)} %queries.1, bf16[256,512]{1,0:T(8,128)(2,1)} %keys.3, bf16[256,1024]{1,0:T(8,128)(2,1)} %values.3, ...), custom_call_target="tpu_custom_call" | custom-call | tf_op jit(solution)/shard_map/cell/pallas_call | solution.py:210
  63.8 3.6 %convolution_convert_fusion.2 = bf16[256,2048]{1,0:T(8,128)(2,1)S(1)} fusion(bf16[256,1024]{1,0:T(8,128)(2,1)} %cell.1, bf16[1024,2048]{1,0:T(8,128)(2,1)} %param.26), kind=kOutput, calls=%fused_computation.2 | convolution fusion | flops 1074266112 | bytes 5767168 | tf_op jit(solution)/shard_map/dot_general | solution.py:279
  67.4 1.0 copy-done.5
  68.6 0.4 convolution_compare_fusion
  69.0 1.5 collective-permute-done
  70.6 1.5 fusion.11
  72.1 1.3 convolution_convert_fusion.1
  73.5 96.9 %all_to_all.20 = bf16[32,32,2048]{2,1,0:T(8,128)(2,1)S(1)} all-to-all(bf16[32,32,2048]{2,1,0:T(8,128)(2,1)S(1)} %bitcast.41), channel_id=1, replica_groups=mesh['sp'=16,'tp'=2] {'sp','tp'}, dimensions={0} | all-to-all | bytes 8388608 | tf_op jit(solution)/shard_map/all_to_all | solution.py:298
  170.4 2.0 copy-done.1
  172.3 3.7 %fusion.3 = f32[1024,512]{1,0:T(8,128)} fusion(bf16[1024,2048]{1,0:T(8,128)(2,1)S(1)} %bitcast.43, bf16[1,2048,512]{2,1,0:T(8,128)(2,1)S(1)} %copy-done.11), kind=kOutput, calls=%fused_computation.8 | convolution fusion | flops 2147483648 | bytes 8388608 | tf_op jit(solution)/shard_map/dot_general | solution.py:252
  176.0 10.1 %convolution_convert_fusion = bf16[1024,2048]{1,0:T(8,128)(2,1)} fusion(bf16[1,512,2048]{2,1,0:T(8,128)(2,1)S(1)} %copy-done, f32[1024,512]{1,0:T(8,128)} %fusion.3, bf16[1024,2048]{1,0:T(8,128)(2,1)} %bitcast.44, bf16[1,2048,512]{2,1,0:T(8,128)(2,1)} %param.31), kind=kOutput, calls=%fused_computation | convolution fusion | flops 4300210176 | bytes 14680064 | tf_op jit(solution)/shard_map/dot_general | solution.py:254
  186.1 3.8 %all-to-all-start.3 = ((bf16[32,32,2048]{2,1,0:T(8,128)(2,1)}), bf16[32,32,2048]{2,1,0:T(8,128)(2,1)}, u32[]{:S(2)}, u32[]{:S(2)}) async-start(bf16[32,32,2048]{2,1,0:T(8,128)(2,1)} %bitcast.42), calls=%async_computation.3 | async-start | bytes 8388608 | tf_op jit(solution)/shard_map/all_to_all | solution.py:306
  190.0 0.4 convolution_select_fusion
  190.4 2.1 fusion.19
  192.5 4.2 %convolution_add_fusion.1 = f32[128,2048]{1,0:T(8,128)} fusion(bf16[512,2048]{1,0:T(8,128)(2,1)} %param.30, bf16[128,2048]{1,0:T(8,128)(2,1)S(1)} %get-tuple-element.6, bf16[2048,512]{1,0:T(8,128)(2,1)} %param.29, f32[2048]{0:T(1024)S(1)} %copy-done.7, f32[128]{0:T(128)S(1)} %add_rsqrt_fusion, f32[128,512]{1,0:T(8,128)S(1)} %fusion.19), kind=kOutput, calls=%fused_computation.5 | convolution fusion | flops 538836992 | bytes 6038016 | tf_op jit(solution)/shard_map/dot_general | solution.py:254
  196.7 86.9 %all-to-all-done.3 = bf16[32,32,2048]{2,1,0:T(8,128)(2,1)} async-done(((bf16[32,32,2048]{2,1,0:T(8,128)(2,1)}), bf16[32,32,2048]{2,1,0:T(8,128)(2,1)}, u32[]{:S(2)}, u32[]{:S(2)}) %all-to-all-start.3) | async-done | bytes 4194336 | tf_op jit(solution)/shard_map/all_to_all | solution.py:306
  283.6 3.0 %fusion.31 = f32[128,2048]{1,0:T(8,128)S(1)} fusion(bf16[1024,2048]{1,0:T(8,128)(2,1)} %bitcast.12, f32[128,1024]{1,0:T(8,128)S(1)} %convolution_select_fusion), kind=kOutput, calls=%fused_computation.35 | convolution fusion | flops 537133056 | bytes 5767168 | tf_op jit(solution)/shard_map/dot_general | solution.py:311
  286.6 3.8 %fusion.1 = bf16[128,2048]{1,0:T(8,128)(2,1)} fusion(f32[128,2048]{1,0:T(8,128)S(1)} %copy-done.2, f32[128,2048]{1,0:T(8,128)S(1)} %fusion.31, bf16[1024,2048]{1,0:T(8,128)(2,1)} %bitcast.12, f32[128,1024]{1,0:T(8,128)S(1)} %convolution_select_fusion), kind=kOutput, calls=%fused_computation.6 | convolution fusion | flops 538050560 | bytes 7340032 | tf_op jit(solution)/shard_map/dot_general | solution.py:311
  (29 shorter events, 0.2 us)
Async XLA Ops:
  0.0 176.0 %copy-start = (bf16[1,512,2048]{2,1,0:T(8,128)(2,1)S(1)}, bf16[1,512,2048]{2,1,0:T(8,128)(2,1)}, u32[]{:S(2)}) copy-start(bf16[1,512,2048]{2,1,0:T(8,128)(2,1)} %param.33) | copy-start | bytes 6291460
  6.5 34.2 %copy-start.8 = (f32[2,256,4]{1,2,0:T(4,128)S(1)}, f32[2,256,4]{1,2,0:T(4,128)}, u32[]{:S(2)}) copy-start(f32[2,256,4]{1,2,0:T(4,128)} %param.23) | copy-start | bytes 24580
  6.5 25.8 %all-to-all-start = ((bf16[16,80,256]{2,1,0:T(8,128)(2,1)}), bf16[16,80,256]{2,1,0:T(8,128)(2,1)S(1)}, u32[]{:S(2)}, u32[]{:S(2)}) async-start(bf16[16,80,256]{2,1,0:T(8,128)(2,1)} %summary.1), calls=%async_computation | async-start | bytes 1310720 | tf_op jit(solution)/shard_map/all_to_all | solution.py:201
  32.4 0.9 copy-start.3
  35.6 20.9 %all-to-all-start.1 = ((bf16[16,80,256]{2,1,0:T(8,128)(2,1)}), bf16[16,80,256]{2,1,0:T(8,128)(2,1)S(1)}, u32[]{:S(2)}, u32[]{:S(2)}) async-start(bf16[16,80,256]{2,1,0:T(8,128)(2,1)} %prefix.1), calls=%async_computation.1 | async-start | bytes 1310720 | tf_op jit(solution)/shard_map/all_to_all | solution.py:209
  56.6 0.9 copy-start.4
  63.8 4.8 %copy-start.9 = (s32[128,4]{0,1:T(4,128)S(1)}, s32[128,4]{0,1:T(4,128)}, u32[]{:S(2)}) copy-start(s32[128,4]{0,1:T(4,128)} %param.34) | copy-start | bytes 6148
  67.4 1.0 copy-start.5
  68.4 2.2 copy-start.6
  68.4 3.7 %copy-start.7 = (f32[2048]{0:T(1024)S(1)}, f32[2048]{0:T(1024)}, u32[]{:S(2)}) copy-start(f32[2048]{0:T(1024)} %param.27) | copy-start | bytes 24580
  68.4 2.1 collective-permute-start
  73.5 98.9 %copy-start.11 = (bf16[1,2048,512]{2,1,0:T(8,128)(2,1)S(1)}, bf16[1,2048,512]{2,1,0:T(8,128)(2,1)}, u32[]{:S(2)}) copy-start(bf16[1,2048,512]{2,1,0:T(8,128)(2,1)} %param.32) | copy-start | bytes 6291460
  170.4 2.0 copy-start.1
  186.1 3.8 %copy-start.10 = (f32[128,4]{0,1:T(4,128)S(1)}, f32[128,4]{0,1:T(4,128)}, u32[]{:S(2)}) copy-start(f32[128,4]{0,1:T(4,128)} %param.35) | copy-start | bytes 6148
  186.1 97.5 %all-to-all-start.3 = ((bf16[32,32,2048]{2,1,0:T(8,128)(2,1)}), bf16[32,32,2048]{2,1,0:T(8,128)(2,1)}, u32[]{:S(2)}, u32[]{:S(2)}) async-start(bf16[32,32,2048]{2,1,0:T(8,128)(2,1)} %bitcast.42), calls=%async_computation.3 | async-start | bytes 8388608 | tf_op jit(solution)/shard_map/all_to_all | solution.py:306
  283.6 3.0 %copy-start.2 = (f32[128,2048]{1,0:T(8,128)S(1)}, f32[128,2048]{1,0:T(8,128)}, u32[]{:S(2)}) copy-start(f32[128,2048]{1,0:T(8,128)} %convolution_add_fusion.1) | copy-start | bytes 3145732
